TPU v7x, 32 devices: a whole 2x2x4 slice. The times are simulated.
32 devices in a mesh: grp: 2 (over x), ep: 16 (over z, y, core).
Axes of the slice: x: 2, y: 2, z: 4, core: 2. Of those that a mesh axis runs over, the one named last changes fastest.
Arguments:
- resid: bfloat16 [384, 2048], P(('grp', 'ep')), parts along dimension 0, may hold values from -6 to 6
- norm_gains: float32 [4, 2048], replicated, may hold values from 0.1 to 1.9
- w_query: bfloat16 [2048, 1024], P(None, 'ep'), may hold values from -0.125 to 0.125
- w_key: bfloat16 [2048, 1024], P(None, 'ep'), may hold values from -0.125 to 0.125
- w_value: bfloat16 [2048, 1024], P(None, 'ep'), may hold values from -0.125 to 0.125
- w_outgate: bfloat16 [2048, 1024], P(None, 'ep'), may hold values from -0.125 to 0.125
- w_igate: bfloat16 [2048, 8], replicated, may hold values from -0.125 to 0.125
- w_fgate: bfloat16 [2048, 8], replicated, may hold values from -0.125 to 0.125
- igate_bias: float32 [8], replicated, may hold values from -1 to 1
- fgate_bias: float32 [8], replicated, may hold values from -1 to 5
- state_matrix: float32 [384, 8, 128, 128], P(('grp', 'ep')), parts along dimension 0, may hold values from -0.8 to 0.8
- state_norm: float32 [384, 8, 128], P(('grp', 'ep')), parts along dimension 0, may hold values from -2.4 to 2.4
- state_max: float32 [384, 8], P(('grp', 'ep')), parts along dimension 0, may hold values from -1 to 1
- w_mix_out: bfloat16 [1024, 2048], replicated, may hold values from -0.1875 to 0.1875
- routes: int32 [384, 2], P(('grp', 'ep')), parts along dimension 0, may hold values from 0 to 15, all different within a row; in each aligned block of 12 rows (0 to 11, 12 to 23, ...) at most 2 rows name the same one
- route_scores: bfloat16 [384, 2], P(('grp', 'ep')), parts along dimension 0, may hold values from 0.099609375 to 1
- expert_gate: bfloat16 [16, 2048, 512], P('ep'), may hold values from -0.125 to 0.125
- expert_up: bfloat16 [16, 2048, 512], P('ep'), may hold values from -0.125 to 0.125
- expert_down: bfloat16 [16, 512, 2048], P('ep'), may hold values from -0.25 to 0.25
- dense_gate: bfloat16 [2048, 8192], P(None, 'ep'), may hold values from -0.125 to 0.125
- dense_up: bfloat16 [2048, 8192], P(None, 'ep'), may hold values from -0.125 to 0.125
- dense_down: bfloat16 [8192, 2048], P('ep'), may hold values from -0.0625 to 0.0625
- branch_weight: bfloat16 [2048], replicated, may hold values from -0.125 to 0.125
Outputs:
- out_stream: bfloat16 [384, 2048], P(('grp', 'ep')), parts along dimension 0
- new_matrix: float32 [384, 8, 128, 128], P(('grp', 'ep')), parts along dimension 0
- new_norm: float32 [384, 8, 128], P(('grp', 'ep')), parts along dimension 0
- new_max: float32 [384, 8], P(('grp', 'ep')), parts along dimension 0
There are 2 independent parts, one for each index of `grp`. A program takes and returns all parts, laid end to end along the dimension named above; an argument that names none is the same for every part. Nothing has to cross between parts.
Inputs may be any that keep to these rules, and one draw needn't show every extreme that they name: `routes`: each row names 2 different experts. In each aligned block of 12 rows (the rows of one device) no expert is named by more than 2 rows, a bound that some block reaches.
All inputs are finite; a program needn't handle non-finite values.
Results may differ from a plain program's by a relative error of at most 0.015.
Values may be sent and summed in bfloat16 or wider, within the bound.
A program may use at most 128 MiB of HBM per device.

v0:
```python
import jax
import jax.numpy as jnp
from jax import lax
from jax.sharding import PartitionSpec as P

CAP = 2


def rms_scale(values, gains):
    return values * lax.rsqrt(jnp.mean(values * values, axis=-1, keepdims=True) + 1e-06) * gains


def expert_batch(picked, gate_matrix, up_matrix, down_matrix):
    gate_out = jnp.einsum("jrd,jdf->jrf", picked, gate_matrix, preferred_element_type=jnp.float32)
    up_out = jnp.einsum("jrd,jdf->jrf", picked, up_matrix, preferred_element_type=jnp.float32)
    hidden = (jax.nn.silu(gate_out) * up_out).astype(jnp.bfloat16)
    return jnp.einsum(
        "jrf,jfd->jrd", hidden, down_matrix, preferred_element_type=jnp.float32
    ).astype(jnp.bfloat16)


def route_tables(routes, route_scores, expert_ids):
    onehot = (routes[:, :, None] == expert_ids[None, None, :]).astype(jnp.float32)
    scores = route_scores.astype(jnp.float32)
    shares = scores / jnp.sum(scores, axis=-1, keepdims=True)
    weights = jnp.sum(shares[:, :, None] * onehot, axis=1)
    hit_count = jnp.sum(onehot, axis=1)
    return (weights, hit_count)


def exchanged_experts(
    branch_in, routes, route_scores, expert_gate, expert_up, expert_down, devices_ep
):
    experts = expert_gate.shape[0] * devices_ep
    weights, hit_count = route_tables(routes, route_scores, jnp.arange(experts, dtype=jnp.int32))
    hit_int = hit_count.astype(jnp.int32)
    rank_index = jnp.cumsum(hit_int, axis=0) - hit_int
    slot_range = jnp.arange(CAP, dtype=jnp.int32)
    chosen = (
        (rank_index.T[:, None, :] == slot_range[None, :, None]) & (hit_count.T[:, None, :] > 0.5)
    ).astype(jnp.float32)
    outgoing = jnp.einsum(
        "ect,td->ecd", chosen.astype(jnp.bfloat16), branch_in, preferred_element_type=jnp.float32
    ).astype(jnp.bfloat16)
    incoming = lax.all_to_all(outgoing, "ep", split_axis=0, concat_axis=1, tiled=True)
    produced = expert_batch(incoming, expert_gate, expert_up, expert_down)
    returned = lax.all_to_all(produced, "ep", split_axis=1, concat_axis=0, tiled=True)
    weighted = chosen * weights.T[:, None, :]
    each_expert = jnp.einsum(
        "ect,ecd->etd", weighted, returned.astype(jnp.float32), precision=lax.Precision.HIGHEST
    )
    return jnp.sum(each_expert.astype(jnp.bfloat16).astype(jnp.float32), axis=0)


def local(
    resid,
    norm_gains,
    w_query,
    w_key,
    w_value,
    w_outgate,
    w_igate,
    w_fgate,
    igate_bias,
    fgate_bias,
    state_matrix,
    state_norm,
    state_max,
    w_mix_out,
    routes,
    route_scores,
    expert_gate,
    expert_up,
    expert_down,
    dense_gate,
    dense_up,
    dense_down,
    branch_weight,
):
    seqs_local = resid.shape[0]
    heads = state_matrix.shape[1]
    head_size = state_matrix.shape[2]
    devices_ep = lax.axis_size("ep")
    resid32 = resid.astype(jnp.float32)
    normed = rms_scale(resid32, norm_gains[0]).astype(jnp.bfloat16)
    row_piece = lax.all_gather(normed, "ep", axis=0, tiled=True)
    projected = jnp.stack(
        [
            jnp.dot(row_piece, matrix, preferred_element_type=jnp.float32).astype(jnp.bfloat16)
            for matrix in (w_query, w_key, w_value, w_outgate)
        ],
        axis=1,
    )
    own_proj = lax.all_to_all(projected, "ep", split_axis=0, concat_axis=2, tiled=True)
    head_shape = (seqs_local, heads, head_size)
    query = own_proj[:, 0].astype(jnp.float32).reshape(head_shape)
    key_heads = own_proj[:, 1].astype(jnp.float32).reshape(head_shape) * head_size ** (-0.5)
    value_heads = own_proj[:, 2].astype(jnp.float32).reshape(head_shape)
    outgate = own_proj[:, 3].astype(jnp.float32).reshape(head_shape)
    ipre = jnp.dot(normed, w_igate, preferred_element_type=jnp.float32) + igate_bias
    fpre = jnp.dot(normed, w_fgate, preferred_element_type=jnp.float32) + fgate_bias
    logf = jax.nn.log_sigmoid(fpre)
    new_max = jnp.maximum(ipre, logf + state_max)
    keep_gain = jnp.exp(logf + state_max - new_max)
    write_gain = jnp.exp(ipre - new_max)
    new_matrix = (
        keep_gain[:, :, None, None] * state_matrix
        + write_gain[:, :, None, None] * value_heads[:, :, :, None] * key_heads[:, :, None, :]
    )
    new_norm = keep_gain[:, :, None] * state_norm + write_gain[:, :, None] * key_heads
    numer = jnp.einsum("shed,shd->she", new_matrix, query, precision=lax.Precision.HIGHEST)
    denom = jnp.sum(new_norm * query, axis=-1)
    cell = numer / jnp.maximum(jnp.abs(denom), 1.0)[:, :, None]
    gated = (
        (jax.nn.sigmoid(outgate) * cell).reshape(seqs_local, heads * head_size).astype(jnp.bfloat16)
    )
    mixed = jnp.dot(gated, w_mix_out, preferred_element_type=jnp.float32)
    middle = resid32 + rms_scale(mixed, norm_gains[1])
    branch_in = rms_scale(middle, norm_gains[2]).astype(jnp.bfloat16)
    all_rows = lax.all_gather(branch_in, "ep", axis=0, tiled=True)
    moe_own = exchanged_experts(
        branch_in, routes, route_scores, expert_gate, expert_up, expert_down, devices_ep
    )
    gate_out = jnp.dot(all_rows, dense_gate, preferred_element_type=jnp.float32)
    up_out = jnp.dot(all_rows, dense_up, preferred_element_type=jnp.float32)
    hidden = (jax.nn.silu(gate_out) * up_out).astype(jnp.bfloat16)
    logit = jnp.dot(all_rows, branch_weight, preferred_element_type=jnp.float32)
    summed = lax.psum_scatter(
        (
            jnp.dot(hidden, dense_down, preferred_element_type=jnp.float32)
            * jax.nn.sigmoid(logit)[:, None]
        ).astype(jnp.bfloat16),
        "ep",
        scatter_dimension=0,
        tiled=True,
    ).astype(jnp.float32)
    combined = moe_own + summed
    out_stream = (middle + rms_scale(combined, norm_gains[3])).astype(jnp.bfloat16)
    return (out_stream, new_matrix, new_norm, new_max)


def solution(mesh):
    placed = (
        P(("grp", "ep"), None),
        P(),
        P(None, "ep"),
        P(None, "ep"),
        P(None, "ep"),
        P(None, "ep"),
        P(),
        P(),
        P(),
        P(),
        P(("grp", "ep"), None, None, None),
        P(("grp", "ep"), None, None),
        P(("grp", "ep"), None),
        P(),
        P(("grp", "ep"), None),
        P(("grp", "ep"), None),
        P("ep", None, None),
        P("ep", None, None),
        P("ep", None, None),
        P(None, "ep"),
        P(None, "ep"),
        P("ep", None),
        P(),
    )
    return jax.shard_map(
        local,
        mesh=mesh,
        in_specs=placed,
        out_specs=(
            P(("grp", "ep"), None),
            P(("grp", "ep"), None, None, None),
            P(("grp", "ep"), None, None),
            P(("grp", "ep"), None),
        ),
        check_vma=False,
    )
```

profile of v0, /device:TPU:17, one launch (start us, length us, event | category | flops | bytes accessed | tf_op | source)
XLA Modules:
  0.0 161.0 jit_solution(14762901746730829710)
XLA Ops:
  0.7 1.0 fusion.62
  1.7 1.0 fusion.30
  2.6 1.0 fusion.61
  3.6 21.5 %all-gather = bf16[16,12,2048]{2,1,0:T(8,128)(2,1)} all-gather(bf16[1,12,2048]{2,1,0:T(8,128)(2,1)S(1)} %fusion.61), channel_id=1, replica_groups=mesh['grp'=2,'ep'=16] {'ep'}, dimensions={0}, use_global_device_ids=true | all-gather | bytes 835584 | tf_op jit(solution)/shard_map/all_gather | solution.py:86
  25.1 1.3 reshape.139
  26.5 0.4 fusion.17
  26.9 0.4 fusion.18
  27.4 0.4 fusion.19
  27.8 0.4 fusion.20
  28.4 0.8 reshape.151
  29.2 8.6 %all-to-all-start = ((bf16[16,2,1536]{2,1,0:T(2,128)(2,1)}), bf16[16,2,1536]{2,1,0:T(2,128)(2,1)S(1)}, u32[]{:S(2)}, u32[]{:S(2)}) async-start(bf16[16,2,1536]{2,1,0:T(2,128)(2,1)} %reshape.151), calls=%async_computation | async-start | bytes 196608 | tf_op jit(solution)/shard_map/all_to_all | solution.py:94
  38.2 0.2 fusion.54
  38.4 0.2 broadcast_multiply_fusion.2
  39.2 3.3 %all-to-all-done = bf16[16,2,1536]{2,1,0:T(2,128)(2,1)S(1)} async-done(((bf16[16,2,1536]{2,1,0:T(2,128)(2,1)}), bf16[16,2,1536]{2,1,0:T(2,128)(2,1)S(1)}, u32[]{:S(2)}, u32[]{:S(2)}) %all-to-all-start) | async-done | bytes 98336 | tf_op jit(solution)/shard_map/all_to_all | solution.py:94
  42.7 0.2 all_to_all.32
  42.9 0.2 slice_reduce_fusion
  43.3 0.7 multiply_reduce_fusion.3
  44.0 4.5 %multiply_add_fusion = f32[12,8,128,128]{3,2,1,0:T(8,128)S(1)} fusion(f32[12,8,128,128]{3,2,1,0:T(8,128)} %param.33, f32[12,8,128]{2,1,0:T(8,128)S(1)} %get-tuple-element.14, f32[12,8,128]{2,1,0:T(8,128)S(1)} %get-tuple-element.21, f32[12,8]{1,0:T(8,128)S(1)} %copy.78), kind=kLoop, calls=%fused_computation | loop fusion | flops 4718592 | bytes 12681600 | tf_op jit(solution)/shard_map/add | solution.py:107
  48.5 5.0 %fusion.43 = f32[12,8,1,128]{3,2,1,0:T(1,128)S(1)} fusion(f32[12,8,128,128]{3,2,1,0:T(8,128)S(1)} %multiply_add_fusion, bf16[12,4,1024]{2,1,0:T(4,128)(2,1)S(1)} %all_to_all.32), kind=kOutput, calls=%fused_computation.61 | convolution fusion | flops 18874368 | bytes 6389760 | tf_op jit(solution)/shard_map/shed,shd->she/dot_general | solution.py:111
  53.6 0.8 multiply_reduce_fusion.2
  54.4 0.2 multiply_reduce_fusion.1
  54.8 22.2 %all-gather.1 = bf16[16,12,2048]{2,1,0:T(8,128)(2,1)} all-gather(bf16[1,12,2048]{2,1,0:T(8,128)(2,1)S(1)} %fusion.58), channel_id=1, replica_groups=mesh['grp'=2,'ep'=16] {'ep'}, dimensions={0}, use_global_device_ids=true | all-gather | bytes 835584 | tf_op jit(solution)/shard_map/all_gather | solution.py:120
  77.0 1.3 reshape.141
  78.3 2.9 %fusion.63 = f32[192,512]{1,0:T(8,128)} fusion(bf16[192,2048]{1,0:T(8,128)(2,1)S(1)} %reshape.141, bf16[2048,512]{1,0:T(8,128)(2,1)} %param.42), kind=kOutput, calls=%fused_computation.106 | convolution fusion | flops 402653184 | bytes 3276800 | tf_op jit(solution)/shard_map/dot_general | solution.py:124
  81.2 0.3 fusion.64
  81.6 0.3 convolution_convert_fusion.2
  81.8 0.8 copy.88
  82.6 6.1 %all-to-all-start.1 = ((bf16[16,2,2048]{2,1,0:T(2,128)(2,1)}), bf16[16,2,2048]{2,1,0:T(2,128)(2,1)S(1)}, u32[]{:S(2)}, u32[]{:S(2)}) async-start(bf16[16,2,2048]{2,1,0:T(2,128)(2,1)} %copy.88), calls=%async_computation.1 | async-start | bytes 262144 | tf_op jit(solution)/shard_map/all_to_all | solution.py:45
  88.7 3.6 %fusion.2 = bf16[192,2048]{1,0:T(8,128)(2,1)} fusion(bf16[512,2048]{1,0:T(8,128)(2,1)S(1)} %copy-done, bf16[192,2048]{1,0:T(8,128)(2,1)S(1)} %reshape.141, bf16[2048,512]{1,0:T(8,128)(2,1)} %param.43, f32[192]{0:T(256)S(1)} %add_divide_fusion, f32[192,512]{1,0:T(8,128)} %fusion.63), kind=kOutput, calls=%fused_computation.4 | convolution fusion | flops 806682624 | bytes 6161152 | tf_op jit(solution)/shard_map/dot_general | solution.py:130
  92.3 1.8 %all-to-all-done.1 = bf16[16,2,2048]{2,1,0:T(2,128)(2,1)S(1)} async-done(((bf16[16,2,2048]{2,1,0:T(2,128)(2,1)}), bf16[16,2,2048]{2,1,0:T(2,128)(2,1)S(1)}, u32[]{:S(2)}, u32[]{:S(2)}) %all-to-all-start.1) | async-done | bytes 131104 | tf_op jit(solution)/shard_map/all_to_all | solution.py:45
  94.2 2.0 %fusion.7 = f32[32,512]{1,0:T(8,128)S(1)} fusion(bf16[32,2048]{1,0:T(8,128)(2,1)S(1)} %reshape.130, bf16[1,2048,512]{2,1,0:T(8,128)(2,1)} %param.39), kind=kOutput, calls=%fused_computation.11 | convolution fusion | flops 67108864 | bytes 2293760 | tf_op jit(solution)/shard_map/jrd,jdf->jrf/dot_general | solution.py:14
  96.2 3.2 %fusion.3 = bf16[1,32,2048]{2,1,0:T(8,128)(2,1)S(1)} fusion(bf16[1,512,2048]{2,1,0:T(8,128)(2,1)} %param.41, bf16[32,2048]{1,0:T(8,128)(2,1)S(1)} %reshape.130, bf16[1,2048,512]{2,1,0:T(8,128)(2,1)} %param.40, f32[32,512]{1,0:T(8,128)S(1)} %fusion.7), kind=kOutput, calls=%fused_computation.7 | convolution fusion | flops 134381568 | bytes 4521984 | tf_op jit(solution)/shard_map/jrf,jfd->jrd/dot_general | solution.py:17
  99.4 0.2 copy.98
  99.7 0.5 broadcast.129
  100.2 1.4 reduce.4
  101.5 0.8 reshape.153
  102.3 6.0 %all-to-all-start.2 = ((bf16[16,2,2048]{2,1,0:T(2,128)(2,1)}), bf16[16,2,2048]{2,1,0:T(2,128)(2,1)S(1)}, u32[]{:S(2)}, u32[]{:S(2)}) async-start(bf16[16,2,2048]{2,1,0:T(2,128)(2,1)} %reshape.153), calls=%async_computation.2 | async-start | bytes 262144 | tf_op jit(solution)/shard_map/all_to_all | solution.py:47
  108.3 28.7 %fusion = bf16[16,2048]{1,0:T(8,128)(2,1)S(1)} fusion(bf16[192,2048]{1,0:T(8,128)(2,1)S(1)} %copy-done.4), kind=kCustom, calls=%all-reduce-scatter | all-reduce-scatter fusion | flops 524289 | bytes 852480
  137.0 2.6 %collective-permute-start = (bf16[16,2048]{1,0:T(8,128)(2,1)S(1)}, bf16[16,2048]{1,0:T(8,128)(2,1)S(1)}, u32[]{:S(2)}, u32[]{:S(2)}) collective-permute-start(bf16[16,2048]{1,0:T(8,128)(2,1)S(1)} %fusion), channel_id=1, source_target_pairs={{0,1},{1,2},{2,3},{3,4},{4,5},{5,6},{6,7},{7,8},{8,9},{9,10},{10,1... | collective-permute-start | bytes 196616
  139.6 5.4 %collective-permute-start.1 = (bf16[16,2048]{1,0:T(8,128)(2,1)S(1)}, bf16[16,2048]{1,0:T(8,128)(2,1)S(1)}, u32[]{:S(2)}, u32[]{:S(2)}) collective-permute-start(bf16[16,2048]{1,0:T(8,128)(2,1)S(1)} %fusion), channel_id=1, source_target_pairs={{0,2},{1,3},{2,4},{3,5},{4,6},{5,7},{6,8},{7,9},{8,10},{9,11},{10,... | collective-permute-start | bytes 196616
  145.0 7.3 %collective-permute-start.2 = (bf16[16,2048]{1,0:T(8,128)(2,1)S(1)}, bf16[16,2048]{1,0:T(8,128)(2,1)S(1)}, u32[]{:S(2)}, u32[]{:S(2)}) collective-permute-start(bf16[16,2048]{1,0:T(8,128)(2,1)S(1)} %fusion), channel_id=1, source_target_pairs={{0,3},{1,4},{2,5},{3,6},{4,7},{5,8},{6,9},{7,10},{8,11},{9,12},{10... | collective-permute-start | bytes 196616
  152.3 1.9 %collective-permute-start.3 = (bf16[12,2048]{1,0:T(8,128)(2,1)S(1)}, bf16[12,2048]{1,0:T(8,128)(2,1)S(1)}, u32[]{:S(2)}, u32[]{:S(2)}) collective-permute-start(bf16[12,2048]{1,0:T(8,128)(2,1)S(1)} %slice.36), channel_id=1, source_target_pairs={{0,4},{1,5},{2,6},{3,7},{4,8},{5,9},{6,10},{7,11},{8,12},{9,13},{1... | collective-permute-start | bytes 147464
  154.3 0.6 dynamic-slice.4
  155.6 1.8 %collective-permute-done.3 = bf16[12,2048]{1,0:T(8,128)(2,1)S(1)} collective-permute-done((bf16[12,2048]{1,0:T(8,128)(2,1)S(1)}, bf16[12,2048]{1,0:T(8,128)(2,1)S(1)}, u32[]{:S(2)}, u32[]{:S(2)}) %collective-permute-start.3) | collective-permute-done | bytes 49184
  157.3 0.7 concatenate
  158.2 0.7 bitcast_reduce_fusion
  159.1 1.1 fusion.9
  160.3 0.7 add_convert_fusion
  (83 shorter events, 2.4 us)
Async XLA Ops:
  0.6 88.1 %copy-start = (bf16[512,2048]{1,0:T(8,128)(2,1)S(1)}, bf16[512,2048]{1,0:T(8,128)(2,1)}, u32[]{:S(2)}) copy-start(bf16[512,2048]{1,0:T(8,128)(2,1)} %param.44) | copy-start | bytes 6291460
  0.6 25.8 %copy-start.5 = (bf16[2048,64]{0,1:T(8,128)(2,1)S(1)}, bf16[2048,64]{0,1:T(8,128)(2,1)}, u32[]{:S(2)}) copy-start(bf16[2048,64]{0,1:T(8,128)(2,1)} %param.25) | copy-start | bytes 786436
  2.6 24.2 %copy-start.6 = (bf16[2048,64]{0,1:T(8,128)(2,1)S(1)}, bf16[2048,64]{0,1:T(8,128)(2,1)}, u32[]{:S(2)}) copy-start(bf16[2048,64]{0,1:T(8,128)(2,1)} %param.26) | copy-start | bytes 786436
  26.4 1.0 copy-start.7
  26.4 1.3 copy-start.8
  26.8 10.9 %copy-start.14 = (bf16[12,2]{0,1:T(2,128)(2,1)S(1)}, bf16[12,2]{0,1:T(2,128)(2,1)}, u32[]{:S(2)}) copy-start(bf16[12,2]{0,1:T(2,128)(2,1)} %param.38) | copy-start | bytes 148
  26.9 11.1 %copy-start.12 = (s32[12,2]{0,1:T(2,128)S(1)}, s32[12,2]{0,1:T(2,128)}, u32[]{:S(2)}) copy-start(s32[12,2]{0,1:T(2,128)} %param.37) | copy-start | bytes 292
  26.9 11.3 %copy-start.3 = (bf16[12,2048]{1,0:T(8,128)(2,1)S(1)}, bf16[12,2048]{1,0:T(8,128)(2,1)}, u32[]{:S(2)}) copy-start(bf16[12,2048]{1,0:T(8,128)(2,1)} %param.23) | copy-start | bytes 147460
  26.9 11.3 %copy-start.15 = (bf16[2048,8]{0,1:T(8,128)(2,1)S(1)}, bf16[2048,8]{0,1:T(8,128)(2,1)}, u32[]{:S(2)}) copy-start(bf16[2048,8]{0,1:T(8,128)(2,1)} %param.30) | copy-start | bytes 98308
  26.9 11.3 %copy-start.17 = (f32[12,8]{0,1:T(8,128)S(1)}, f32[12,8]{0,1:T(8,128)}, u32[]{:S(2)}) copy-start(f32[12,8]{0,1:T(8,128)} %param.35) | copy-start | bytes 1156
  26.9 11.3 %copy-start.18 = (f32[8]{0:T(128)S(1)}, f32[8]{0:T(128)}, u32[]{:S(2)}) copy-start(f32[8]{0:T(128)} %param.32) | copy-start | bytes 100
  26.9 11.5 %copy-start.16 = (bf16[2048,8]{0,1:T(8,128)(2,1)S(1)}, bf16[2048,8]{0,1:T(8,128)(2,1)}, u32[]{:S(2)}) copy-start(bf16[2048,8]{0,1:T(8,128)(2,1)} %param.29) | copy-start | bytes 98308
  26.9 11.5 %copy-start.19 = (f32[8]{0:T(128)S(1)}, f32[8]{0:T(128)}, u32[]{:S(2)}) copy-start(f32[8]{0:T(128)} %param.31) | copy-start | bytes 100
  27.4 11.5 %copy-start.10 = (bf16[2048]{0:T(1024)(128)(2,1)S(1)}, bf16[2048]{0:T(1024)(128)(2,1)}, u32[]{:S(2)}) copy-start(bf16[2048]{0:T(1024)(128)(2,1)} %param.45) | copy-start | bytes 12292
  27.8 15.5 %copy-start.9 = (f32[12,8,128]{2,1,0:T(8,128)S(1)}, f32[12,8,128]{2,1,0:T(8,128)}, u32[]{:S(2)}) copy-start(f32[12,8,128]{2,1,0:T(8,128)} %param.34) | copy-start | bytes 147460
  29.2 13.3 %all-to-all-start = ((bf16[16,2,1536]{2,1,0:T(2,128)(2,1)}), bf16[16,2,1536]{2,1,0:T(2,128)(2,1)S(1)}, u32[]{:S(2)}, u32[]{:S(2)}) async-start(bf16[16,2,1536]{2,1,0:T(2,128)(2,1)} %reshape.151), calls=%async_computation | async-start | bytes 196608 | tf_op jit(solution)/shard_map/all_to_all | solution.py:94
  38.6 9.8 %copy-start.11 = (f32[12,8]{0,1:T(8,128)}, f32[12,8]{0,1:T(8,128)S(1)}, u32[]{:S(2)}) copy-start(f32[12,8]{0,1:T(8,128)S(1)} %get-tuple-element.10) | copy-start | bytes 1156
  48.5 5.0 %copy-start.1 = (f32[12,8,128,128]{3,2,1,0:T(8,128)}, f32[12,8,128,128]{3,2,1,0:T(8,128)S(1)}, u32[]{:S(2)}) copy-start(f32[12,8,128,128]{3,2,1,0:T(8,128)S(1)} %multiply_add_fusion) | copy-start | bytes 18874372
  48.5 5.1 %copy-start.2 = (bf16[1024,2048]{1,0:T(8,128)(2,1)S(1)}, bf16[1024,2048]{1,0:T(8,128)(2,1)}, u32[]{:S(2)}) copy-start(bf16[1024,2048]{1,0:T(8,128)(2,1)} %param.36) | copy-start | bytes 12582916
  82.6 11.5 %all-to-all-start.1 = ((bf16[16,2,2048]{2,1,0:T(2,128)(2,1)}), bf16[16,2,2048]{2,1,0:T(2,128)(2,1)S(1)}, u32[]{:S(2)}, u32[]{:S(2)}) async-start(bf16[16,2,2048]{2,1,0:T(2,128)(2,1)} %copy.88), calls=%async_computation.1 | async-start | bytes 262144 | tf_op jit(solution)/shard_map/all_to_all | solution.py:45
  96.2 12.1 %copy-start.4 = (bf16[192,2048]{1,0:T(8,128)(2,1)S(1)}, bf16[192,2048]{1,0:T(8,128)(2,1)}, u32[]{:S(2)}) copy-start(bf16[192,2048]{1,0:T(8,128)(2,1)} %fusion.2) | copy-start | bytes 2359300
  99.4 54.9 %copy-start.13 = (u32[32]{0:T(128)S(1)}, u32[32]{0:T(128)}, u32[]{:S(2)}) copy-start(u32[32]{0:T(128)} %constant.42) | copy-start | bytes 388
  102.3 55.8 %all-to-all-start.2 = ((bf16[16,2,2048]{2,1,0:T(2,128)(2,1)}), bf16[16,2,2048]{2,1,0:T(2,128)(2,1)S(1)}, u32[]{:S(2)}, u32[]{:S(2)}) async-start(bf16[16,2,2048]{2,1,0:T(2,128)(2,1)} %reshape.153), calls=%async_computation.2 | async-start | bytes 262144 | tf_op jit(solution)/shard_map/all_to_all | solution.py:47
  137.0 20.4 %collective-permute-start = (bf16[16,2048]{1,0:T(8,128)(2,1)S(1)}, bf16[16,2048]{1,0:T(8,128)(2,1)S(1)}, u32[]{:S(2)}, u32[]{:S(2)}) collective-permute-start(bf16[16,2048]{1,0:T(8,128)(2,1)S(1)} %fusion), channel_id=1, source_target_pairs={{0,1},{1,2},{2,3},{3,4},{4,5},{5,6},{6,7},{7,8},{8,9},{9,10},{10,1... | collective-permute-start | bytes 196616
  139.6 17.7 %collective-permute-start.1 = (bf16[16,2048]{1,0:T(8,128)(2,1)S(1)}, bf16[16,2048]{1,0:T(8,128)(2,1)S(1)}, u32[]{:S(2)}, u32[]{:S(2)}) collective-permute-start(bf16[16,2048]{1,0:T(8,128)(2,1)S(1)} %fusion), channel_id=1, source_target_pairs={{0,2},{1,3},{2,4},{3,5},{4,6},{5,7},{6,8},{7,9},{8,10},{9,11},{10,... | collective-permute-start | bytes 196616
  145.0 12.3 %collective-permute-start.2 = (bf16[16,2048]{1,0:T(8,128)(2,1)S(1)}, bf16[16,2048]{1,0:T(8,128)(2,1)S(1)}, u32[]{:S(2)}, u32[]{:S(2)}) collective-permute-start(bf16[16,2048]{1,0:T(8,128)(2,1)S(1)} %fusion), channel_id=1, source_target_pairs={{0,3},{1,4},{2,5},{3,6},{4,7},{5,8},{6,9},{7,10},{8,11},{9,12},{10... | collective-permute-start | bytes 196616
  152.3 5.0 %collective-permute-start.3 = (bf16[12,2048]{1,0:T(8,128)(2,1)S(1)}, bf16[12,2048]{1,0:T(8,128)(2,1)S(1)}, u32[]{:S(2)}, u32[]{:S(2)}) collective-permute-start(bf16[12,2048]{1,0:T(8,128)(2,1)S(1)} %slice.36), channel_id=1, source_target_pairs={{0,4},{1,5},{2,6},{3,7},{4,8},{5,9},{6,10},{7,11},{8,12},{9,13},{1... | collective-permute-start | bytes 147464
where the time goes:
time: 162 us; the launch traced here: 161 us
  blocking collectives  72.4 us (45%)
  starting transfers between devices  37.8 us (23%)
  matrix products  21.1 us (13%)
  local copies, waits for them, and re-layouts  10.5 us (6%)
  other arithmetic  10.4 us (6%)
  waiting for transfers between devices  6.9 us (4%)
  between operations  1.84 us (1%)
    unnamed x1, blocking collectives  28.7 us
    all_gather x1, blocking collectives, local(): all_rows = lax.all_gather(branch_in, 'ep', axis=0, tiled=True)  22.2 us
    all_gather x1, blocking collectives, local(): row_piece = lax.all_gather(normed, 'ep', axis=0, tiled=True)  21.5 us
    unnamed x4, starting transfers between devices  17.2 us
    all_to_all x1, starting transfers between devices, local(): lax.all_to_all(projected, 'ep', split_axis=0, concat_axis=2, tiled=True)  8.56 us
    unnamed x55, local copies, waits for them, and re-layouts  6.65 us
    all_to_all x1, starting transfers between devices, exchanged_experts(): lax.all_to_all(outgoing, 'ep', split_axis=0, concat_axis=1, tiled=True)  6.08 us
    all_to_all x1, starting transfers between devices, exchanged_experts(): lax.all_to_all(produced, 'ep', split_axis=1, concat_axis=0, tiled=True)  5.97 us
  transfers between devices with their start and end apart: 7, of which 3 were waited for; matrix products, arithmetic and copies ran while one was open for 22% of the time, Pallas kernels for 0%

commit v1 on v0

--- a/solution.py
+++ b/solution.py
@@ -83,7 +83,9 @@
     devices_ep = lax.axis_size("ep")
     resid32 = resid.astype(jnp.float32)
     normed = rms_scale(resid32, norm_gains[0]).astype(jnp.bfloat16)
-    row_piece = lax.all_gather(normed, "ep", axis=0, tiled=True)
+    row_piece = jnp.concatenate(
+        lax.all_to_all(jnp.stack([normed] * lax.axis_size("ep")), "ep", 0, 0), axis=0
+    )
     projected = jnp.stack(
         [
             jnp.dot(row_piece, matrix, preferred_element_type=jnp.float32).astype(jnp.bfloat16)

time: 162 us -> 169 us (1.043)
  waiting for transfers between devices: 6.9 us -> 31.7 us
  blocking collectives: 72.4 us -> 50.7 us
  starting transfers between devices: 37.8 us -> 41.3 us
    all_to_all x0 -> x1, waiting for transfers between devices: none -> 23.4 us  [local(): lax.all_to_all(jnp.stack([normed] * lax.axis_size('ep')), 'ep', 0, 0)]
    all_gather x1 -> x0, blocking collectives: 21.5 us -> none  [local(): row_piece = lax.all_gather(normed, 'ep', axis=0, tiled=True)]
    all_to_all x0 -> x1, starting transfers between devices: none -> 6.6 us  [local(): lax.all_to_all(jnp.stack([normed] * lax.axis_size('ep')), 'ep', 0, 0)]
    all_to_all x1, starting transfers between devices: 8.56 us -> 5.12 us  [local(): lax.all_to_all(projected, 'ep', split_axis=0, concat_axis=2, tiled=True)]
    unnamed x55 -> x54, local copies, waits for them, and re-layouts: 6.65 us -> 5.46 us
  transfers between devices with their start and end apart: 7 -> 8, of which waited for: 3 -> 4; matrix products, arithmetic and copies ran while one was open for 22% -> 21% of each run, Pallas kernels for 0% -> 0%
where the time goes in v1:
time: 169 us
  blocking collectives  50.7 us (30%)
  starting transfers between devices  41.3 us (24%)
  waiting for transfers between devices  31.7 us (19%)
  matrix products  21 us (12%)
  local copies, waits for them, and re-layouts  11.7 us (7%)
  other arithmetic  10.4 us (6%)
  between operations  1.82 us (1%)
    unnamed x1, blocking collectives  28.7 us
    all_to_all x1, waiting for transfers between devices, local(): lax.all_to_all(jnp.stack([normed] * lax.axis_size('ep')), 'ep', 0, 0)  23.4 us
    all_gather x1, blocking collectives, local(): all_rows = lax.all_gather(branch_in, 'ep', axis=0, tiled=True)  22 us
    unnamed x4, starting transfers between devices  17.2 us
    all_to_all x1, starting transfers between devices, local(): lax.all_to_all(jnp.stack([normed] * lax.axis_size('ep')), 'ep', 0, 0)  6.6 us
    all_to_all x1, starting transfers between devices, exchanged_experts(): lax.all_to_all(outgoing, 'ep', split_axis=0, concat_axis=1, tiled=True)  6.38 us
    all_to_all x1, starting transfers between devices, exchanged_experts(): lax.all_to_all(produced, 'ep', split_axis=1, concat_axis=0, tiled=True)  5.97 us
    unnamed x54, local copies, waits for them, and re-layouts  5.46 us
  transfers between devices with their start and end apart: 8, of which 4 were waited for; matrix products, arithmetic and copies ran while one was open for 21% of the time, Pallas kernels for 0%

profile of v1, /device:TPU:17, one launch (start us, length us, event | category | flops | bytes accessed | tf_op | source)
XLA Modules:
  0.0 168.6 jit_solution(10048920712850791843)
XLA Ops:
  0.7 1.0 fusion.59
  1.7 1.0 fusion.30
  2.7 0.9 fusion.32
  3.6 1.1 stack.12
  4.7 6.6 %all-to-all-start = ((bf16[16,12,2048]{2,1,0:T(8,128)(2,1)}), bf16[16,12,2048]{2,1,0:T(8,128)(2,1)}, u32[]{:S(2)}, u32[]{:S(2)}) async-start(bf16[16,12,2048]{2,1,0:T(8,128)(2,1)} %stack.12), calls=%async_computation | async-start | bytes 2097152 | tf_op jit(solution)/shard_map/all_to_all | solution.py:87
  12.5 23.4 %all-to-all-done = bf16[16,12,2048]{2,1,0:T(8,128)(2,1)} async-done(((bf16[16,12,2048]{2,1,0:T(8,128)(2,1)}), bf16[16,12,2048]{2,1,0:T(8,128)(2,1)}, u32[]{:S(2)}, u32[]{:S(2)}) %all-to-all-start) | async-done | bytes 786464 | tf_op jit(solution)/shard_map/all_to_all | solution.py:87
  36.0 1.3 reshape.134
  37.3 0.4 fusion.17
  37.7 0.4 fusion.18
  38.3 0.4 fusion.19
  38.7 0.4 fusion.20
  39.3 0.8 reshape.155
  40.1 5.1 %all-to-all-start.1 = ((bf16[16,2,1536]{2,1,0:T(2,128)(2,1)}), bf16[16,2,1536]{2,1,0:T(2,128)(2,1)S(1)}, u32[]{:S(2)}, u32[]{:S(2)}) async-start(bf16[16,2,1536]{2,1,0:T(2,128)(2,1)} %reshape.155), calls=%async_computation.1 | async-start | bytes 196608 | tf_op jit(solution)/shard_map/all_to_all | solution.py:96
  45.2 4.7 %all-to-all-done.1 = bf16[16,2,1536]{2,1,0:T(2,128)(2,1)S(1)} async-done(((bf16[16,2,1536]{2,1,0:T(2,128)(2,1)}), bf16[16,2,1536]{2,1,0:T(2,128)(2,1)S(1)}, u32[]{:S(2)}, u32[]{:S(2)}) %all-to-all-start.1) | async-done | bytes 98336 | tf_op jit(solution)/shard_map/all_to_all | solution.py:96
  50.2 0.2 all_to_all.36
  50.3 0.2 slice_reduce_fusion
  50.7 0.7 multiply_reduce_fusion.3
  51.4 4.5 %multiply_add_fusion = f32[12,8,128,128]{3,2,1,0:T(8,128)S(1)} fusion(f32[12,8,128,128]{3,2,1,0:T(8,128)} %param.33, f32[12,8,128]{2,1,0:T(8,128)S(1)} %get-tuple-element.14, f32[12,8,128]{2,1,0:T(8,128)S(1)} %get-tuple-element.21, f32[12,8]{1,0:T(8,128)S(1)} %copy.78), kind=kLoop, calls=%fused_computation | loop fusion | flops 4718592 | bytes 12681600 | tf_op jit(solution)/shard_map/add | solution.py:109
  55.9 5.0 %fusion.43 = f32[12,8,1,128]{3,2,1,0:T(1,128)S(1)} fusion(f32[12,8,128,128]{3,2,1,0:T(8,128)S(1)} %multiply_add_fusion, bf16[12,4,1024]{2,1,0:T(4,128)(2,1)S(1)} %all_to_all.36), kind=kOutput, calls=%fused_computation.61 | convolution fusion | flops 18874368 | bytes 6389760 | tf_op jit(solution)/shard_map/shed,shd->she/dot_general | solution.py:113
  61.1 0.8 multiply_reduce_fusion.2
  61.9 0.2 multiply_reduce_fusion.1
  62.2 22.0 %all-gather = bf16[16,12,2048]{2,1,0:T(8,128)(2,1)} all-gather(bf16[1,12,2048]{2,1,0:T(8,128)(2,1)S(1)} %fusion.58), channel_id=1, replica_groups=mesh['grp'=2,'ep'=16] {'ep'}, dimensions={0}, use_global_device_ids=true | all-gather | bytes 835584 | tf_op jit(solution)/shard_map/all_gather | solution.py:122
  84.3 1.3 reshape.145
  85.6 2.9 %fusion.60 = f32[192,512]{1,0:T(8,128)} fusion(bf16[192,2048]{1,0:T(8,128)(2,1)S(1)} %reshape.145, bf16[2048,512]{1,0:T(8,128)(2,1)} %param.42), kind=kOutput, calls=%fused_computation.105 | convolution fusion | flops 402653184 | bytes 3276800 | tf_op jit(solution)/shard_map/dot_general | solution.py:126
  88.5 0.3 fusion.61
  88.8 0.3 convolution_convert_fusion.2
  89.1 0.8 copy.88
  89.9 6.4 %all-to-all-start.2 = ((bf16[16,2,2048]{2,1,0:T(2,128)(2,1)}), bf16[16,2,2048]{2,1,0:T(2,128)(2,1)S(1)}, u32[]{:S(2)}, u32[]{:S(2)}) async-start(bf16[16,2,2048]{2,1,0:T(2,128)(2,1)} %copy.88), calls=%async_computation.2 | async-start | bytes 262144 | tf_op jit(solution)/shard_map/all_to_all | solution.py:45
  96.2 3.6 %fusion.2 = bf16[192,2048]{1,0:T(8,128)(2,1)} fusion(bf16[512,2048]{1,0:T(8,128)(2,1)S(1)} %copy-done, bf16[192,2048]{1,0:T(8,128)(2,1)S(1)} %reshape.145, bf16[2048,512]{1,0:T(8,128)(2,1)} %param.43, f32[192]{0:T(256)S(1)} %add_divide_fusion, f32[192,512]{1,0:T(8,128)} %fusion.60), kind=kOutput, calls=%fused_computation.4 | convolution fusion | flops 806682624 | bytes 6161152 | tf_op jit(solution)/shard_map/dot_general | solution.py:132
  99.9 1.8 %all-to-all-done.2 = bf16[16,2,2048]{2,1,0:T(2,128)(2,1)S(1)} async-done(((bf16[16,2,2048]{2,1,0:T(2,128)(2,1)}), bf16[16,2,2048]{2,1,0:T(2,128)(2,1)S(1)}, u32[]{:S(2)}, u32[]{:S(2)}) %all-to-all-start.2) | async-done | bytes 131104 | tf_op jit(solution)/shard_map/all_to_all | solution.py:45
  101.7 2.0 %fusion.7 = f32[32,512]{1,0:T(8,128)S(1)} fusion(bf16[32,2048]{1,0:T(8,128)(2,1)S(1)} %reshape.136, bf16[1,2048,512]{2,1,0:T(8,128)(2,1)} %param.39), kind=kOutput, calls=%fused_computation.11 | convolution fusion | flops 67108864 | bytes 2293760 | tf_op jit(solution)/shard_map/jrd,jdf->jrf/dot_general | solution.py:14
  103.8 3.2 %fusion.3 = bf16[1,32,2048]{2,1,0:T(8,128)(2,1)S(1)} fusion(bf16[1,512,2048]{2,1,0:T(8,128)(2,1)} %param.41, bf16[32,2048]{1,0:T(8,128)(2,1)S(1)} %reshape.136, bf16[1,2048,512]{2,1,0:T(8,128)(2,1)} %param.40, f32[32,512]{1,0:T(8,128)S(1)} %fusion.7), kind=kOutput, calls=%fused_computation.7 | convolution fusion | flops 134381568 | bytes 4521984 | tf_op jit(solution)/shard_map/jrf,jfd->jrd/dot_general | solution.py:17
  107.0 0.2 copy.98
  107.2 0.5 broadcast.131
  107.7 1.4 reduce.4
  109.1 0.8 reshape.157
  109.8 6.0 %all-to-all-start.3 = ((bf16[16,2,2048]{2,1,0:T(2,128)(2,1)}), bf16[16,2,2048]{2,1,0:T(2,128)(2,1)S(1)}, u32[]{:S(2)}, u32[]{:S(2)}) async-start(bf16[16,2,2048]{2,1,0:T(2,128)(2,1)} %reshape.157), calls=%async_computation.3 | async-start | bytes 262144 | tf_op jit(solution)/shard_map/all_to_all | solution.py:47
  115.8 28.7 %fusion = bf16[16,2048]{1,0:T(8,128)(2,1)S(1)} fusion(bf16[192,2048]{1,0:T(8,128)(2,1)S(1)} %copy-done.4), kind=kCustom, calls=%all-reduce-scatter | all-reduce-scatter fusion | flops 524289 | bytes 852480
  144.5 2.6 %collective-permute-start = (bf16[16,2048]{1,0:T(8,128)(2,1)S(1)}, bf16[16,2048]{1,0:T(8,128)(2,1)S(1)}, u32[]{:S(2)}, u32[]{:S(2)}) collective-permute-start(bf16[16,2048]{1,0:T(8,128)(2,1)S(1)} %fusion), channel_id=1, source_target_pairs={{0,1},{1,2},{2,3},{3,4},{4,5},{5,6},{6,7},{7,8},{8,9},{9,10},{10,1... | collective-permute-start | bytes 196616
  147.2 5.4 %collective-permute-start.1 = (bf16[16,2048]{1,0:T(8,128)(2,1)S(1)}, bf16[16,2048]{1,0:T(8,128)(2,1)S(1)}, u32[]{:S(2)}, u32[]{:S(2)}) collective-permute-start(bf16[16,2048]{1,0:T(8,128)(2,1)S(1)} %fusion), channel_id=1, source_target_pairs={{0,2},{1,3},{2,4},{3,5},{4,6},{5,7},{6,8},{7,9},{8,10},{9,11},{10,... | collective-permute-start | bytes 196616
  152.6 7.3 %collective-permute-start.2 = (bf16[16,2048]{1,0:T(8,128)(2,1)S(1)}, bf16[16,2048]{1,0:T(8,128)(2,1)S(1)}, u32[]{:S(2)}, u32[]{:S(2)}) collective-permute-start(bf16[16,2048]{1,0:T(8,128)(2,1)S(1)} %fusion), channel_id=1, source_target_pairs={{0,3},{1,4},{2,5},{3,6},{4,7},{5,8},{6,9},{7,10},{8,11},{9,12},{10... | collective-permute-start | bytes 196616
  159.9 1.9 %collective-permute-start.3 = (bf16[12,2048]{1,0:T(8,128)(2,1)S(1)}, bf16[12,2048]{1,0:T(8,128)(2,1)S(1)}, u32[]{:S(2)}, u32[]{:S(2)}) collective-permute-start(bf16[12,2048]{1,0:T(8,128)(2,1)S(1)} %slice.36), channel_id=1, source_target_pairs={{0,4},{1,5},{2,6},{3,7},{4,8},{5,9},{6,10},{7,11},{8,12},{9,13},{1... | collective-permute-start | bytes 147464
  161.9 0.6 dynamic-slice.4
  163.1 1.8 %collective-permute-done.3 = bf16[12,2048]{1,0:T(8,128)(2,1)S(1)} collective-permute-done((bf16[12,2048]{1,0:T(8,128)(2,1)S(1)}, bf16[12,2048]{1,0:T(8,128)(2,1)S(1)}, u32[]{:S(2)}, u32[]{:S(2)}) %collective-permute-start.3) | collective-permute-done | bytes 49184
  164.9 0.7 concatenate
  165.8 0.7 bitcast_reduce_fusion
  166.6 1.1 fusion.9
  167.8 0.7 add_convert_fusion
  (85 shorter events, 2.8 us)
Async XLA Ops:
  0.6 95.6 %copy-start = (bf16[512,2048]{1,0:T(8,128)(2,1)S(1)}, bf16[512,2048]{1,0:T(8,128)(2,1)}, u32[]{:S(2)}) copy-start(bf16[512,2048]{1,0:T(8,128)(2,1)} %param.44) | copy-start | bytes 6291460
  0.7 10.7 %copy-start.15 = (bf16[2048,8]{0,1:T(8,128)(2,1)S(1)}, bf16[2048,8]{0,1:T(8,128)(2,1)}, u32[]{:S(2)}) copy-start(bf16[2048,8]{0,1:T(8,128)(2,1)} %param.30) | copy-start | bytes 98308
  0.7 10.7 %copy-start.18 = (f32[8]{0:T(128)S(1)}, f32[8]{0:T(128)}, u32[]{:S(2)}) copy-start(f32[8]{0:T(128)} %param.32) | copy-start | bytes 100
  0.7 10.7 %copy-start.17 = (f32[12,8]{0,1:T(8,128)S(1)}, f32[12,8]{0,1:T(8,128)}, u32[]{:S(2)}) copy-start(f32[12,8]{0,1:T(8,128)} %param.35) | copy-start | bytes 1156
  0.7 10.8 %copy-start.16 = (bf16[2048,8]{0,1:T(8,128)(2,1)S(1)}, bf16[2048,8]{0,1:T(8,128)(2,1)}, u32[]{:S(2)}) copy-start(bf16[2048,8]{0,1:T(8,128)(2,1)} %param.29) | copy-start | bytes 98308
  0.7 10.8 %copy-start.19 = (f32[8]{0:T(128)S(1)}, f32[8]{0:T(128)}, u32[]{:S(2)}) copy-start(f32[8]{0:T(128)} %param.31) | copy-start | bytes 100
  0.7 11.2 %copy-start.10 = (bf16[2048]{0:T(1024)(128)(2,1)S(1)}, bf16[2048]{0:T(1024)(128)(2,1)}, u32[]{:S(2)}) copy-start(bf16[2048]{0:T(1024)(128)(2,1)} %param.45) | copy-start | bytes 12292
  0.7 11.2 %copy-start.14 = (bf16[12,2]{0,1:T(2,128)(2,1)S(1)}, bf16[12,2]{0,1:T(2,128)(2,1)}, u32[]{:S(2)}) copy-start(bf16[12,2]{0,1:T(2,128)(2,1)} %param.38) | copy-start | bytes 148
  0.7 11.4 %copy-start.12 = (s32[12,2]{0,1:T(2,128)S(1)}, s32[12,2]{0,1:T(2,128)}, u32[]{:S(2)}) copy-start(s32[12,2]{0,1:T(2,128)} %param.37) | copy-start | bytes 292
  4.7 32.6 %copy-start.5 = (bf16[2048,64]{0,1:T(8,128)(2,1)S(1)}, bf16[2048,64]{0,1:T(8,128)(2,1)}, u32[]{:S(2)}) copy-start(bf16[2048,64]{0,1:T(8,128)(2,1)} %param.25) | copy-start | bytes 786436
  4.7 31.3 %all-to-all-start = ((bf16[16,12,2048]{2,1,0:T(8,128)(2,1)}), bf16[16,12,2048]{2,1,0:T(8,128)(2,1)}, u32[]{:S(2)}, u32[]{:S(2)}) async-start(bf16[16,12,2048]{2,1,0:T(8,128)(2,1)} %stack.12), calls=%async_computation | async-start | bytes 2097152 | tf_op jit(solution)/shard_map/all_to_all | solution.py:87
  11.3 26.4 %copy-start.6 = (bf16[2048,64]{0,1:T(8,128)(2,1)S(1)}, bf16[2048,64]{0,1:T(8,128)(2,1)}, u32[]{:S(2)}) copy-start(bf16[2048,64]{0,1:T(8,128)(2,1)} %param.26) | copy-start | bytes 786436
  11.7 26.4 %copy-start.11 = (f32[12,8]{0,1:T(8,128)}, f32[12,8]{0,1:T(8,128)S(1)}, u32[]{:S(2)}) copy-start(f32[12,8]{0,1:T(8,128)S(1)} %get-tuple-element.10) | copy-start | bytes 1156
  37.3 1.0 copy-start.7
  37.3 1.3 copy-start.8
  38.3 12.4 %copy-start.9 = (f32[12,8,128]{2,1,0:T(8,128)S(1)}, f32[12,8,128]{2,1,0:T(8,128)}, u32[]{:S(2)}) copy-start(f32[12,8,128]{2,1,0:T(8,128)} %param.34) | copy-start | bytes 147460
  40.1 9.9 %all-to-all-start.1 = ((bf16[16,2,1536]{2,1,0:T(2,128)(2,1)}), bf16[16,2,1536]{2,1,0:T(2,128)(2,1)S(1)}, u32[]{:S(2)}, u32[]{:S(2)}) async-start(bf16[16,2,1536]{2,1,0:T(2,128)(2,1)} %reshape.155), calls=%async_computation.1 | async-start | bytes 196608 | tf_op jit(solution)/shard_map/all_to_all | solution.py:96
  55.9 5.0 %copy-start.1 = (f32[12,8,128,128]{3,2,1,0:T(8,128)}, f32[12,8,128,128]{3,2,1,0:T(8,128)S(1)}, u32[]{:S(2)}) copy-start(f32[12,8,128,128]{3,2,1,0:T(8,128)S(1)} %multiply_add_fusion) | copy-start | bytes 18874372
  55.9 5.1 %copy-start.2 = (bf16[1024,2048]{1,0:T(8,128)(2,1)S(1)}, bf16[1024,2048]{1,0:T(8,128)(2,1)}, u32[]{:S(2)}) copy-start(bf16[1024,2048]{1,0:T(8,128)(2,1)} %param.36) | copy-start | bytes 12582916
  61.1 0.8 copy-start.3
  89.9 11.8 %all-to-all-start.2 = ((bf16[16,2,2048]{2,1,0:T(2,128)(2,1)}), bf16[16,2,2048]{2,1,0:T(2,128)(2,1)S(1)}, u32[]{:S(2)}, u32[]{:S(2)}) async-start(bf16[16,2,2048]{2,1,0:T(2,128)(2,1)} %copy.88), calls=%async_computation.2 | async-start | bytes 262144 | tf_op jit(solution)/shard_map/all_to_all | solution.py:45
  103.8 12.1 %copy-start.4 = (bf16[192,2048]{1,0:T(8,128)(2,1)S(1)}, bf16[192,2048]{1,0:T(8,128)(2,1)}, u32[]{:S(2)}) copy-start(bf16[192,2048]{1,0:T(8,128)(2,1)} %fusion.2) | copy-start | bytes 2359300
  107.0 54.9 %copy-start.13 = (u32[32]{0:T(128)S(1)}, u32[32]{0:T(128)}, u32[]{:S(2)}) copy-start(u32[32]{0:T(128)} %constant.42) | copy-start | bytes 388
  109.8 55.8 %all-to-all-start.3 = ((bf16[16,2,2048]{2,1,0:T(2,128)(2,1)}), bf16[16,2,2048]{2,1,0:T(2,128)(2,1)S(1)}, u32[]{:S(2)}, u32[]{:S(2)}) async-start(bf16[16,2,2048]{2,1,0:T(2,128)(2,1)} %reshape.157), calls=%async_computation.3 | async-start | bytes 262144 | tf_op jit(solution)/shard_map/all_to_all | solution.py:47
  144.5 20.4 %collective-permute-start = (bf16[16,2048]{1,0:T(8,128)(2,1)S(1)}, bf16[16,2048]{1,0:T(8,128)(2,1)S(1)}, u32[]{:S(2)}, u32[]{:S(2)}) collective-permute-start(bf16[16,2048]{1,0:T(8,128)(2,1)S(1)} %fusion), channel_id=1, source_target_pairs={{0,1},{1,2},{2,3},{3,4},{4,5},{5,6},{6,7},{7,8},{8,9},{9,10},{10,1... | collective-permute-start | bytes 196616
  147.2 17.7 %collective-permute-start.1 = (bf16[16,2048]{1,0:T(8,128)(2,1)S(1)}, bf16[16,2048]{1,0:T(8,128)(2,1)S(1)}, u32[]{:S(2)}, u32[]{:S(2)}) collective-permute-start(bf16[16,2048]{1,0:T(8,128)(2,1)S(1)} %fusion), channel_id=1, source_target_pairs={{0,2},{1,3},{2,4},{3,5},{4,6},{5,7},{6,8},{7,9},{8,10},{9,11},{10,... | collective-permute-start | bytes 196616
  152.6 12.3 %collective-permute-start.2 = (bf16[16,2048]{1,0:T(8,128)(2,1)S(1)}, bf16[16,2048]{1,0:T(8,128)(2,1)S(1)}, u32[]{:S(2)}, u32[]{:S(2)}) collective-permute-start(bf16[16,2048]{1,0:T(8,128)(2,1)S(1)} %fusion), channel_id=1, source_target_pairs={{0,3},{1,4},{2,5},{3,6},{4,7},{5,8},{6,9},{7,10},{8,11},{9,12},{10... | collective-permute-start | bytes 196616
  159.9 5.0 %collective-permute-start.3 = (bf16[12,2048]{1,0:T(8,128)(2,1)S(1)}, bf16[12,2048]{1,0:T(8,128)(2,1)S(1)}, u32[]{:S(2)}, u32[]{:S(2)}) collective-permute-start(bf16[12,2048]{1,0:T(8,128)(2,1)S(1)} %slice.36), channel_id=1, source_target_pairs={{0,4},{1,5},{2,6},{3,7},{4,8},{5,9},{6,10},{7,11},{8,12},{9,13},{1... | collective-permute-start | bytes 147464
